TPU v7x, 1024 devices: a whole 8x8x8 slice. The times are simulated.
1024 devices in a mesh: sp: 16 (over x, core), tp: 64 (over z, y).
Axes of the slice: x: 8, y: 8, z: 8, core: 2. Of those that a mesh axis runs over, the one named last changes fastest.
Arguments:
- latents: bfloat16 [4096, 2048], P(('sp', 'tp')), may hold values from -6 to 6
- context: bfloat16 [1024, 2048], P('sp'), may hold values from -6 to 6
- condition: float32 [2048], P('sp'), may hold values from -12 to 12
- context_condition: float32 [2048], P('sp'), may hold values from -12 to 12
- norm_gain: float32 [2048], replicated, may hold values from 0.1 to 1.9
- shift_weight: bfloat16 [2048, 2048], P('sp', 'tp'), may hold values from -0.09375 to 0.09375
- scale_weight: bfloat16 [2048, 2048], P('sp', 'tp'), may hold values from -0.09375 to 0.09375
- gate_weight: bfloat16 [2048, 2048], P('sp', 'tp'), may hold values from -0.125 to 0.125
- query_weight: bfloat16 [2048, 8192], P(None, 'tp'), may hold values from -0.125 to 0.125
- key_weight: bfloat16 [2048, 8192], P(None, 'tp'), may hold values from -0.125 to 0.125
- value_weight: bfloat16 [2048, 8192], P(None, 'tp'), may hold values from -0.125 to 0.125
- subtract_share: float32 [64], P('tp'), may hold values from 0.3 to 0.8
- head_gain: float32 [128], replicated, may hold values from 0.1 to 1.9
- output_weight: bfloat16 [8192, 2048], P('tp'), may hold values from -0.0625 to 0.0625
Outputs:
- updated: bfloat16 [4096, 2048], P(('sp', 'tp'))
All inputs are finite; a program needn't handle non-finite values.
Results may differ from a plain program's by a relative error of at most 0.013.
Values may be sent and summed in bfloat16 or wider, within the bound.
A program may use at most 32 MiB of HBM per device.

v0:
```python
import jax
import jax.numpy as jnp
from jax import lax
from jax.sharding import PartitionSpec as P

HEAD = 64
VALUE = 128
GRID_W = 64


norm_eps = 1e-06
head_eps = 1e-05
rope_theta = 10000.0
head_scale = 0.8


def copy_for_each(array, axis):
    size = lax.axis_size(axis)
    return lax.all_to_all(
        jnp.broadcast_to(array[None], (size, *array.shape)), axis, 0, 0, tiled=True
    )


def of_everyone(array, axis):
    return copy_for_each(array, axis).sum(axis=0)


def in_order(tiles, dim):
    tiles = jnp.moveaxis(tiles, 0, dim)
    shape = tiles.shape
    return tiles.reshape(*shape[:dim], shape[dim] * shape[dim + 1], *shape[dim + 2 :])


def gather_directly(array, axis, dim):
    tiles = copy_for_each(array, axis)
    return in_order(tiles, dim)


def split_up(array, dim, size):
    before, after = (array.shape[:dim], array.shape[dim + 1 :])
    return jnp.moveaxis(array.reshape(*before, size, -1, *after), dim, 0)


def sent_and_summed(array, axis, dim):
    size = lax.axis_size(axis)
    tiles = lax.all_to_all(split_up(array, dim, size), axis, 0, 0, tiled=True)
    return jnp.sum(tiles, axis=0)


def rotary_tables(positions):
    quarter = HEAD // 4
    inverse = rope_theta ** (-2.0 * jnp.arange(quarter, dtype=jnp.float32) / (HEAD // 2))
    row_angle = (positions // GRID_W).astype(jnp.float32)[:, None] * inverse[None, :]
    column_angle = (positions % GRID_W).astype(jnp.float32)[:, None] * inverse[None, :]
    angles = jnp.concatenate([row_angle, row_angle, column_angle, column_angle], axis=-1)
    return (jnp.cos(angles), jnp.sin(angles))


def rotate(vectors, cosine, sine_table):
    quarter = HEAD // 4
    pieces = vectors.reshape(vectors.shape[:-1] + (2, 2, quarter))
    turned = jnp.concatenate([-pieces[..., 1:, :], pieces[..., :1, :]], axis=-2).reshape(
        vectors.shape
    )
    return vectors * cosine[:, None, :] + turned * sine_table[:, None, :]


def modulate(token_rows, gain_row, shift_row, scale_row):
    widened = token_rows.astype(jnp.float32)
    normed = widened * lax.rsqrt(jnp.mean(widened * widened, axis=-1, keepdims=True) + norm_eps)
    return (normed * gain_row * (1.0 + scale_row) + shift_row).astype(jnp.bfloat16)


def shards(
    latents,
    context,
    condition,
    context_condition,
    norm_gain,
    shift_weight,
    scale_weight,
    gate_weight,
    query_weight,
    key_weight,
    value_weight,
    subtract_share,
    head_gain,
    output_weight,
):
    activated = jax.nn.silu(jnp.stack([condition, context_condition])).astype(jnp.bfloat16)
    partial_terms = jnp.stack(
        [
            jnp.dot(activated, matrix, preferred_element_type=jnp.float32)
            for matrix in (shift_weight, scale_weight, gate_weight)
        ]
    )
    summed = of_everyone(partial_terms, "sp")
    full_terms = gather_directly(summed, "tp", 2)
    shift_terms, scale_terms, gate_terms = (full_terms[0], full_terms[1], full_terms[2])
    pair_weight = jnp.concatenate([key_weight, value_weight], axis=1)
    joined = jnp.concatenate([query_weight, pair_weight], axis=1)
    projected = jnp.dot(
        modulate(gather_directly(latents, "tp", 0), norm_gain, shift_terms[0], scale_terms[0]),
        joined,
        preferred_element_type=jnp.float32,
    )
    local_count = projected.shape[0]
    positions = lax.axis_index("sp") * local_count + jnp.arange(local_count, dtype=jnp.int32)
    cosine, sine_table = rotary_tables(positions)
    queries = rotate(projected[:, :VALUE].reshape(local_count, 2, HEAD), cosine, sine_table)
    queries = queries.reshape(local_count, VALUE).astype(jnp.bfloat16)
    latent_keys = rotate(
        projected[:, VALUE : 2 * VALUE].reshape(local_count, 2, HEAD), cosine, sine_table
    )
    latent_keys = latent_keys.reshape(local_count, VALUE).astype(jnp.bfloat16)
    latent_pairs = jnp.concatenate(
        [latent_keys, projected[:, 2 * VALUE :].astype(jnp.bfloat16)], axis=1
    )
    context_mod = modulate(context, norm_gain, shift_terms[1], scale_terms[1])
    context_pairs = jnp.dot(context_mod, pair_weight, preferred_element_type=jnp.float32).astype(
        jnp.bfloat16
    )
    sent_pairs = jnp.concatenate([latent_pairs, context_pairs], axis=0)
    arrived = lax.all_gather(sent_pairs, "sp", axis=0, tiled=True)
    updated_carry = []
    for which_map in range(2):
        offset = which_map * HEAD
        scores = jnp.einsum(
            "qd,kd->qk",
            queries[:, offset : offset + HEAD],
            arrived[:, offset : offset + HEAD],
            preferred_element_type=jnp.float32,
        ) * HEAD ** (-0.5)
        powers = jnp.exp(scores)
        updated_carry.append(
            jnp.dot(
                powers.astype(jnp.bfloat16), arrived[:, VALUE:], preferred_element_type=jnp.float32
            )
        )
        updated_carry.append(jnp.sum(powers, axis=1, keepdims=True))
    first_sum, first_total, second_sum, second_total = tuple(updated_carry)
    share_value = subtract_share[0]
    difference = first_sum / first_total - share_value * (second_sum / second_total)
    normed = difference * lax.rsqrt(
        jnp.mean(difference * difference, axis=1, keepdims=True) + head_eps
    )
    head_output = (normed * head_gain * head_scale).astype(jnp.bfloat16)
    branch = sent_and_summed(
        jnp.dot(head_output, output_weight, preferred_element_type=jnp.float32), "tp", 0
    )
    return (latents.astype(jnp.float32) + gate_terms[0] * branch).astype(jnp.bfloat16)


def solution(mesh):
    in_specs = (
        P(("sp", "tp"), None),
        P("sp", None),
        P("sp"),
        P("sp"),
        P(),
        P("sp", "tp"),
        P("sp", "tp"),
        P("sp", "tp"),
        P(None, "tp"),
        P(None, "tp"),
        P(None, "tp"),
        P("tp"),
        P(),
        P("tp", None),
    )
    out_specs = P(("sp", "tp"), None)
    return jax.shard_map(shards, mesh=mesh, in_specs=in_specs, out_specs=out_specs, check_vma=False)
```

profile of v0, /device:TPU:1, one launch (start us, length us, event | category | flops | bytes accessed | tf_op | source)
XLA Modules:
  0.0 218.1 jit_solution(6100877642774426645)
XLA Ops:
  6.5 0.9 convolution_bitcast_fusion.1
  7.4 0.9 convolution_bitcast_fusion
  8.3 0.9 convolution_bitcast_fusion.2
  9.3 23.9 %all_to_all.20 = f32[16,1,192]{2,1,0:T(1,128)S(1)} all-to-all(f32[16,1,192]{2,1,0:T(1,128)S(1)} %reshape.261), channel_id=1, replica_groups=mesh['sp'=16,'tp'=64] {'sp'}, dimensions={0} | all-to-all | bytes 24576 | tf_op jit(solution)/shard_map/all_to_all | solution.py:19
  33.7 0.7 reduce.21
  34.8 25.6 %all_to_all.21 = f32[64,1,192]{2,1,0:T(1,128)S(1)} all-to-all(f32[64,1,192]{2,1,0:T(1,128)S(1)} %reshape.263), channel_id=1, replica_groups=mesh['sp'=16,'tp'=64] {'tp'}, dimensions={0} | all-to-all | bytes 98304 | tf_op jit(solution)/shard_map/all_to_all | solution.py:19
  60.4 2.3 %broadcast_in_dim.8 = bf16[64,4,2048]{2,1,0:T(4,128)(2,1)} broadcast(bf16[4,2048]{1,0:T(4,128)(2,1)} %param.14), dimensions={1,2} | broadcast | bytes 1064960 | tf_op jit(solution)/shard_map/broadcast_in_dim | solution.py:20
  62.7 4.8 %all-to-all-start.2 = ((bf16[64,4,2048]{2,1,0:T(4,128)(2,1)}), bf16[64,4,2048]{2,1,0:T(4,128)(2,1)S(1)}, u32[]{:S(2)}, u32[]{:S(2)}) async-start(bf16[64,4,2048]{2,1,0:T(4,128)(2,1)} %broadcast_in_dim.8), calls=%async_computation.2 | async-start | bytes 2097152 | tf_op jit(solution)/shard_map/all_to_all | solution.py:19
  68.2 0.8 reduce.22
  70.3 23.3 %all-to-all-done.2 = bf16[64,4,2048]{2,1,0:T(4,128)(2,1)S(1)} async-done(((bf16[64,4,2048]{2,1,0:T(4,128)(2,1)}), bf16[64,4,2048]{2,1,0:T(4,128)(2,1)S(1)}, u32[]{:S(2)}, u32[]{:S(2)}) %all-to-all-start.2) | async-done | bytes 1048608 | tf_op jit(solution)/shard_map/all_to_all | solution.py:19
  93.6 0.6 multiply_reduce_fusion
  94.3 1.4 reshape.233
  95.8 2.4 %fusion.6 = f32[256,384]{1,0:T(8,128)S(1)} fusion(bf16[2048,128]{1,0:T(8,128)(2,1)S(1)} %copy-done.5, bf16[2048,128]{1,0:T(8,128)(2,1)S(1)} %copy-done.6, bf16[2048,128]{1,0:T(8,128)(2,1)} %param.22, f32[256,2048]{1,0:T(8,128)} %reshape.233, f32[2048]{0:T(1024)S(1)} %add.122, f32[2048]{0:T(1024)S(1)} %add.121, f32[2048]{0:T(1024)S(1)} %copy-done.7, ...), kind=kOutput, calls=%fused_computation.10 | convolution fusion | flops 409993216 | bytes 4088832 | tf_op jit(solution)/shard_map/dot_general | solution.py:102
  98.8 0.7 pad_maximum_fusion
  100.1 38.1 %all-gather.2.cloned.1.call-done = bf16[5120,256]{1,0:T(8,128)(2,1)} async-done(((bf16[320,256]{1,0:T(8,128)(2,1)}), bf16[5120,256]{1,0:T(8,128)(2,1)}) %all-gather.2.cloned.1.call-update) | async-done | bytes 2621456 | tf_op jit(solution)/shard_map/all_gather | solution.py:124
  138.2 2.9 %fusion.74 = (f32[256]{0:T(256)S(1)}, bf16[256,5120]{1,0:T(8,128)(2,1)S(1)}) fusion(bf16[5120,256]{1,0:T(8,128)(2,1)} %all-gather.2.cloned.1.call-done, bf16[256,128]{1,0:T(8,128)(2,1)S(1)} %get-tuple-element.10), kind=kOutput, calls=%fused_computation.97 | convolution fusion | flops 171704064 | bytes 3998720 | tf_op jit(solution)/shard_map/qd,kd->qk/dot_general | solution.py:128
  141.1 1.1 fusion.75
  142.2 1.0 fusion.31
  143.3 1.0 multiply_reduce_fusion.1
  144.4 0.5 fusion.53
  144.9 1.7 reshape.232
  146.6 13.8 %all-to-all-start.3 = ((f32[64,4,2048]{2,1,0:T(4,128)}), f32[64,4,2048]{2,1,0:T(4,128)S(1)}, u32[]{:S(2)}, u32[]{:S(2)}) async-start(f32[64,4,2048]{2,1,0:T(4,128)} %reshape.232), calls=%async_computation.3 | async-start | bytes 4194304 | tf_op jit(solution)/shard_map/all_to_all | solution.py:46
  160.5 49.8 %all-to-all-done.3 = f32[64,4,2048]{2,1,0:T(4,128)S(1)} async-done(((f32[64,4,2048]{2,1,0:T(4,128)}), f32[64,4,2048]{2,1,0:T(4,128)S(1)}, u32[]{:S(2)}, u32[]{:S(2)}) %all-to-all-start.3) | async-done | bytes 2097184 | tf_op jit(solution)/shard_map/all_to_all | solution.py:46
  210.7 0.6 add_convert_fusion.4
  (59 shorter events, 4.0 us)
Async XLA Ops:
  6.5 137.8 %copy-start = (bf16[128,2048]{1,0:T(8,128)(2,1)S(1)}, bf16[128,2048]{1,0:T(8,128)(2,1)}, u32[]{:S(2)}) copy-start(bf16[128,2048]{1,0:T(8,128)(2,1)} %param.27) | copy-start | bytes 1572868
  60.4 7.6 %copy-start.1 = (bf16[64,2048]{1,0:T(8,128)(2,1)S(1)}, bf16[64,2048]{1,0:T(8,128)(2,1)}, u32[]{:S(2)}) copy-start(bf16[64,2048]{1,0:T(8,128)(2,1)} %param.15) | copy-start | bytes 786436
  62.7 7.2 %copy-start.5 = (bf16[2048,128]{1,0:T(8,128)(2,1)S(1)}, bf16[2048,128]{1,0:T(8,128)(2,1)}, u32[]{:S(2)}) copy-start(bf16[2048,128]{1,0:T(8,128)(2,1)} %param.24) | copy-start | bytes 1572868
  62.7 7.2 %copy-start.6 = (bf16[2048,128]{1,0:T(8,128)(2,1)S(1)}, bf16[2048,128]{1,0:T(8,128)(2,1)}, u32[]{:S(2)}) copy-start(bf16[2048,128]{1,0:T(8,128)(2,1)} %param.23) | copy-start | bytes 1572868
  62.7 7.3 %copy-start.7 = (f32[2048]{0:T(1024)S(1)}, f32[2048]{0:T(1024)}, u32[]{:S(2)}) copy-start(f32[2048]{0:T(1024)} %param.18) | copy-start | bytes 24580
  62.7 30.9 %all-to-all-start.2 = ((bf16[64,4,2048]{2,1,0:T(4,128)(2,1)}), bf16[64,4,2048]{2,1,0:T(4,128)(2,1)S(1)}, u32[]{:S(2)}, u32[]{:S(2)}) async-start(bf16[64,4,2048]{2,1,0:T(4,128)(2,1)} %broadcast_in_dim.8), calls=%async_computation.2 | async-start | bytes 2097152 | tf_op jit(solution)/shard_map/all_to_all | solution.py:19
  67.5 70.7 %all-gather.2.cloned.1.call-start = ((), (), s32[]{:S(2)}) async-start(), calls=%async_computation.4 | async-start | bytes 2785280 | tf_op jit(solution)/shard_map/all_gather | solution.py:124
  138.2 2.9 %copy-start.4 = (bf16[5120,256]{1,0:T(8,128)(2,1)S(1)}, bf16[5120,256]{1,0:T(8,128)(2,1)}, u32[]{:S(2)}) copy-start(bf16[5120,256]{1,0:T(8,128)(2,1)} %all-gather.2.cloned.1.call-done) | copy-start | bytes 7864324
  143.3 1.1 copy-start.3
  146.6 63.7 %all-to-all-start.3 = ((f32[64,4,2048]{2,1,0:T(4,128)}), f32[64,4,2048]{2,1,0:T(4,128)S(1)}, u32[]{:S(2)}, u32[]{:S(2)}) async-start(f32[64,4,2048]{2,1,0:T(4,128)} %reshape.232), calls=%async_computation.3 | async-start | bytes 4194304 | tf_op jit(solution)/shard_map/all_to_all | solution.py:46
  160.4 50.3 %copy-start.2 = (bf16[4,2048]{1,0:T(4,128)(2,1)S(1)}, bf16[4,2048]{1,0:T(4,128)(2,1)}, u32[]{:S(2)}) copy-start(bf16[4,2048]{1,0:T(4,128)(2,1)} %param.14) | copy-start | bytes 49156
Sparse Core Ops, SparseCore 0:
  99.6 38.5 all-gather.1
where the time goes:
time: 221 us; the launch traced here: 218 us
  waiting for transfers between devices  111 us (50%)
  blocking collectives  49.5 us (22%)
  starting transfers between devices  18.7 us (8%)
  between operations  14.4 us (7%)
  matrix products  12 us (5%)
  local copies, waits for them, and re-layouts  7.66 us (3%)
  other arithmetic  4.76 us (2%)
    all_to_all x1, waiting for transfers between devices, sent_and_summed(): tiles = lax.all_to_all(split_up(array, dim, size), axis, 0, 0, tiled=True)  49.8 us
    all_to_all x2, blocking collectives, copy_for_each(): lax.all_to_all(jnp.broadcast_to(array[None], (size, *array.shape)), axis,...  49.5 us
    all_gather x1, waiting for transfers between devices, shards(): arrived = lax.all_gather(sent_pairs, 'sp', axis=0, tiled=True)  38.1 us
    all_to_all x1, waiting for transfers between devices, copy_for_each(): lax.all_to_all(jnp.broadcast_to(array[None], (size, *array.shape)), axis,...  23.3 us
    all_to_all x1, starting transfers between devices, sent_and_summed(): tiles = lax.all_to_all(split_up(array, dim, size), axis, 0, 0, tiled=True)  13.8 us
    all_to_all x1, starting transfers between devices, copy_for_each(): lax.all_to_all(jnp.broadcast_to(array[None], (size, *array.shape)), axis,...  4.78 us
  transfers between devices with their start and end apart: 3, of which 3 were waited for; matrix products, arithmetic and copies ran while one was open for 1% of the time, Pallas kernels for 0%

commit v1 on v0

v1 whole, which is shorter than its diff:
```python
import functools

import jax
import jax.numpy as jnp
from jax import lax
from jax.experimental import pallas as pl
from jax.experimental.pallas import tpu as pltpu
from jax.sharding import PartitionSpec as P

MESH = pl.DeviceIdType.MESH
HEAD = 64
VALUE = 128
GRID_W = 64

norm_eps = 1e-06
head_eps = 1e-05
rope_theta = 10000.0
head_scale = 0.8
F32 = jnp.float32
BF16 = jnp.bfloat16


def iota(shape, dim):
    return lax.broadcasted_iota(jnp.int32, shape, dim)


def when(condition, action):
    if isinstance(condition, bool):
        if condition:
            action()
    else:
        pl.when(condition)(action)


def remote(src, dst, send_sem, recv_sem, device):
    return pltpu.make_async_remote_copy(
        src_ref=src,
        dst_ref=dst,
        send_sem=send_sem,
        recv_sem=recv_sem,
        device_id=device,
        device_id_type=MESH,
    )


class Exchange:
    def __init__(self, me, count, device_of, source, target, send_sems, recv_sems):
        self.me, self.count, self.device_of = me, count, device_of
        self.source, self.target = source, target
        self.send_sems, self.recv_sems = send_sems, recv_sems

    def copy(self, step):
        peer = lax.rem(self.me + step, self.count)
        return remote(
            self.source(peer),
            self.target(self.me),
            self.send_sems.at[step],
            self.recv_sems.at[self.me],
            self.device_of(peer),
        )

    def steps(self):
        return sorted(range(1, self.count), key=lambda s: -min(s, self.count - s))

    def start(self):
        for step in self.steps():
            self.copy(step).start()

    def wait_recv(self):
        for step in self.steps():
            peer = lax.rem(self.me + step, self.count)
            remote(
                self.target(peer),
                self.target(peer),
                self.send_sems.at[step],
                self.recv_sems.at[peer],
                self.device_of(peer),
            ).wait_recv()

    def wait_send(self):
        for step in self.steps():
            self.copy(step).wait_send()


class Ring:
    def __init__(self, me, count, device_of, view, pieces, right_sems, left_sems, recv_sems):
        self.me, self.count, self.device_of, self.view = me, count, device_of, view
        self.pieces, self.half = pieces, count // 2
        self.right_sems, self.left_sems, self.recv_sems = right_sems, left_sems, recv_sems

    def source(self, step, right):
        return lax.rem(self.me + self.count + (-step if right else step), self.count)

    def carries(self, step, piece, right):
        mine = (piece < self.pieces // 2) == right if self.pieces > 1 else right
        last = self.half if mine else self.half - 1
        return step <= last

    def copy(self, step, piece, right):
        place = self.view(self.source(step, right), piece)
        peer = lax.rem(self.me + (1 if right else self.count - 1), self.count)
        sems = self.right_sems if right else self.left_sems
        return remote(
            place,
            place,
            sems.at[step, piece],
            self.recv_sems.at[self.source(step, right), piece],
            self.device_of(peer),
        )

    def send(self, step, piece, right):
        when(
            self.carries(step + 1, piece, right),
            lambda: self.copy(step, piece, right).start(),
        )

    def send_own(self, piece):
        self.send(0, piece, True)
        self.send(0, piece, False)

    def arrive(self, step, piece, right, then=None):
        def go():
            self.copy(step, piece, right).wait_recv()
            self.send(step, piece, right)
            if then is not None:
                then(step, piece, right)

        when(self.carries(step, piece, right), go)

    def arrive_step(self, step, then=None):
        for piece in range(self.pieces):
            self.arrive(step, piece, True, then)
            self.arrive(step, piece, False, then)

    def wait_send(self):
        for step in range(self.half):
            for piece in range(self.pieces):
                for right in (True, False):
                    if self.carries(step + 1, piece, right):
                        self.copy(step, piece, right).wait_send()


def kernel(
    sizes,
    lat,
    ctx,
    cond,
    ctx_cond,
    gain,
    shift_w,
    scale_w,
    gate_w,
    query_w,
    key_w,
    value_w,
    share,
    head_gain,
    out_w,
    out,
    weights,
    out_weights,
    spread,
    part,
    line_terms,
    all_terms,
    lat_line,
    lat_flat,
    lat_all,
    modded,
    cosines,
    sines_up,
    sines_down,
    order,
    queries,
    pairs,
    sums,
    totals,
    heads_out,
    heads_in,
    rows_out,
    rows_in,
    local_sems,
    part_send,
    part_recv,
    line_send,
    line_recv,
    all_send,
    all_recv,
    lat_send,
    lat_recv,
    z_right,
    z_left,
    z_recv,
    w_right,
    w_left,
    w_across,
    w_recv,
    x_right,
    x_left,
    x_across,
    x_recv,
    heads_send,
    heads_recv,
    rows_send,
    rows_recv,
):
    nx, ny, nz = sizes
    nsp = 2 * nx
    rows, width = lat.shape
    line_rows = ny * rows
    count = nz * line_rows
    ctx_rows = ctx.shape[0]
    sp, tp = lax.axis_index("sp"), lax.axis_index("tp")
    x, core = sp // 2, lax.rem(sp, 2)
    z, y = tp // ny, lax.rem(tp, ny)
    other_sp = x * 2 + 1 - core
    sibling = {"sp": other_sp, "tp": tp}

    def on_sp(peer):
        return {"sp": peer, "tp": tp}

    def on_x(peer):
        return {"sp": peer * 2 + core, "tp": tp}

    def on_y(peer):
        return {"sp": sp, "tp": z * ny + peer}

    def on_z(peer):
        return {"sp": sp, "tp": peer * ny + y}

    barrier = pltpu.get_barrier_semaphore()
    for me, size, device_of in ((sp, nsp, on_sp), (y, ny, on_y), (z, nz, on_z)):
        for step in range(1, size):
            pl.semaphore_signal(
                barrier,
                inc=1,
                device_id=device_of(lax.rem(me + step, size)),
                device_id_type=MESH,
            )

    own_half = out_w.shape[0] // 2
    half_rows = own_half // 2
    local = [
        pltpu.make_async_copy(matrix, weights.at[:, pl.ds(i * VALUE, VALUE)], local_sems.at[i])
        for i, matrix in enumerate((query_w, key_w, value_w))
    ]
    for half in range(2):
        for piece in range(2):
            local.append(
                pltpu.make_async_copy(
                    out_w.at[pl.ds(half * own_half + piece * half_rows, half_rows)],
                    out_weights.at[y, half, piece],
                    local_sems.at[3 + 2 * half + piece],
                )
            )
    for copy in local:
        copy.start()

    columns = shift_w.shape[1]
    group = 128 // columns
    tiles = ny // group
    raw = jnp.where(iota((8, cond.shape[1]), 0) == 0, cond[...], ctx_cond[...])
    activated = (raw / (1.0 + jnp.exp(-raw))).astype(BF16)
    spread[...] = jnp.zeros_like(spread)
    for kind, matrix in enumerate((shift_w, scale_w, gate_w)):
        term = jnp.dot(activated, matrix[...], preferred_element_type=F32)[0:2]
        for place in range(group):
            spread[2 * kind : 2 * kind + 2, place * columns : (place + 1) * columns] = term
    here = iota((8, 128), 1) // columns == lax.rem(y, group)
    part[sp] = jnp.where(here, spread[...], 0.0)
    lat_line[y] = lat[...]

    pl.semaphore_wait(barrier, nsp - 1 + ny - 1 + nz - 1)

    part_exchange = Exchange(
        sp, nsp, on_sp, lambda peer: part.at[sp], lambda me: part.at[me], part_send, part_recv
    )
    lat_exchange = Exchange(
        y, ny, on_y, lambda peer: lat, lambda me: lat_line.at[me], lat_send, lat_recv
    )
    line_exchange = Exchange(
        y,
        ny,
        on_y,
        lambda peer: line_terms.at[y],
        lambda me: line_terms.at[me],
        line_send,
        line_recv,
    )
    all_exchange = Exchange(
        z, nz, on_z, lambda peer: all_terms.at[z], lambda me: all_terms.at[me], all_send, all_recv
    )
    heads_exchange = Exchange(
        y,
        ny,
        on_y,
        lambda peer: heads_out.at[peer],
        lambda me: heads_in.at[me],
        heads_send,
        heads_recv,
    )
    rows_exchange = Exchange(
        z, nz, on_z, lambda peer: rows_out.at[peer], lambda me: rows_in.at[me], rows_send, rows_recv
    )
    half_line = line_rows // 2
    lat_ring = Ring(
        z,
        nz,
        on_z,
        lambda source, piece: lat_all.at[source, pl.ds(piece * half_line, half_line)],
        2,
        z_right,
        z_left,
        z_recv,
    )
    weight_ring = Ring(
        y,
        ny,
        on_y,
        lambda source, piece: out_weights.at[source, core, piece],
        2,
        w_right,
        w_left,
        w_recv.at[0],
    )

    def weight_across(step, piece, right):
        place = out_weights.at[weight_ring.source(step, right), core, piece]
        return remote(
            place,
            place,
            w_across.at[1 if right else 0, step, piece],
            w_recv.at[1, weight_ring.source(step, right), piece],
            sibling,
        )

    def send_weight_across(step, piece, right):
        weight_across(step, piece, right).start()

    near = [0]
    for step in range(1, lat_ring.half // 2 + 1):
        near += [-step, step]
    far = [d for d in range(-(lat_ring.half - 1), lat_ring.half + 1) if d not in near]
    near_rows, far_rows = len(near) * line_rows, len(far) * line_rows
    bounds = (
        (0, ctx_rows),
        (ctx_rows, near_rows // 2),
        (ctx_rows + near_rows // 2, near_rows // 2),
        (ctx_rows + near_rows, far_rows),
    )

    def pair_view(source, piece):
        first, size = bounds[piece]
        return pairs.at[source, pl.ds(first, size)]

    pair_ring = Ring(
        x,
        nx,
        on_x,
        lambda source, piece: pair_view(source * 2 + core, piece),
        4,
        x_right,
        x_left,
        x_recv.at[0],
    )

    def pair_across(step, piece, right):
        source = pair_ring.source(step, right)
        place = pair_view(source * 2 + core, piece)
        return remote(
            place,
            place,
            x_across.at[1 if right else 0, step, piece],
            x_recv.at[1, source, piece],
            sibling,
        )

    def send_pair_across(step, piece, right):
        pair_across(step, piece, right).start()

    def send_pair(piece):
        pair_ring.send_own(piece)
        send_pair_across(0, piece, True)

    part_exchange.start()
    lat_exchange.start()

    token = iota((count, VALUE), 0)
    lane = iota((count, VALUE), 1)
    position = sp * count + token
    quarter = HEAD // 4
    frequency = jnp.exp(
        lax.rem(lane, quarter).astype(F32) * (-2.0 / (HEAD // 2) * jnp.log(F32(rope_theta)))
    )
    place = jnp.where(
        lax.rem(lane, HEAD) < HEAD // 2, position // GRID_W, lax.rem(position, GRID_W)
    )
    angle = place.astype(F32) * frequency
    cosines[...] = jnp.cos(angle).reshape(cosines.shape)
    sine = jnp.sin(angle)
    even = lax.rem(lane // quarter, 2) == 0
    sines_up[...] = jnp.where(even, -sine, 0.0).reshape(sines_up.shape)
    sines_down[...] = jnp.where(even, 0.0, sine).reshape(sines_down.shape)
    to = iota((count, count), 0)
    source = (lax.rem(to // rows, nz) * ny + to // (rows * nz)) * rows + lax.rem(to, rows)
    order[...] = jnp.where(iota((count, count), 1) == source, 1.0, 0.0).astype(BF16)
    sums[...] = jnp.zeros_like(sums)
    totals[...] = jnp.zeros_like(totals)

    part_exchange.wait_recv()
    total = part[0]
    for i in range(1, nsp):
        total = total + part[i]
    line_terms[y] = total
    line_exchange.start()

    lat_exchange.wait_recv()
    for i in range(ny):
        lat_flat[i * rows : (i + 1) * rows, :] = lat_line[i].astype(F32)
    lat_all[z] = lat_flat[...].astype(BF16)
    for piece in range(2):
        lat_ring.send_own(piece)

    for copy in local:
        copy.wait()
    for piece in range(2):
        weight_ring.send_own(piece)

    line_exchange.wait_recv()
    for tile in range(tiles):
        total = line_terms[tile * group]
        for i in range(1, group):
            total = total + line_terms[tile * group + i]
        all_terms[z, tile] = total
    all_exchange.start()

    first_steps = lat_ring.half // 2
    for step in range(1, first_steps + 1):
        lat_ring.arrive_step(step)

    all_exchange.wait_recv()

    def term(row):
        return jnp.concatenate(
            [all_terms[i, tile, row : row + 1, :] for i in range(nz) for tile in range(tiles)], axis=1
        )

    def modulate(token_rows, which):
        widened = token_rows.astype(F32)
        normed = widened * lax.rsqrt(jnp.mean(widened * widened, axis=-1, keepdims=True) + norm_eps)
        return (normed * (gain[...] * (1.0 + term(2 + which))) + term(which)).astype(BF16)

    modded[0:ctx_rows, :] = modulate(ctx[...], 1)
    pairs[sp, 0:ctx_rows, :] = jnp.dot(
        modded[0:ctx_rows, :], weights[:, VALUE:], preferred_element_type=F32
    ).astype(BF16)
    send_pair(0)

    def project(blocks, first):
        size = len(blocks) * line_rows
        places = [lax.rem(z + d + nz, nz) for d in blocks]
        for i, block in enumerate(places):
            modded[i * line_rows : (i + 1) * line_rows, :] = modulate(lat_all[block], 0)
        projected = jnp.dot(modded[0:size, :], weights[...], preferred_element_type=F32)
        for i, block in enumerate(places):
            piece = projected[i * line_rows : (i + 1) * line_rows]
            cosine, up, down = cosines[block], sines_up[block], sines_down[block]

            def rotate(vectors):
                return (
                    vectors * cosine
                    + pltpu.roll(vectors, VALUE - quarter, 1) * up
                    + pltpu.roll(vectors, quarter, 1) * down
                )

            query = rotate(piece[:, :VALUE]).astype(BF16).astype(F32) * HEAD ** (-0.5)
            low = iota(query.shape, 1) < HEAD
            queries[0, block] = jnp.where(low, query, 0.0).astype(BF16)
            queries[1, block] = jnp.where(low, 0.0, query).astype(BF16)
            here = slice(first + i * line_rows, first + (i + 1) * line_rows)
            pairs[sp, here, 0:VALUE] = rotate(piece[:, VALUE : 2 * VALUE]).astype(BF16)
            pairs[sp, here, VALUE:] = piece[:, 2 * VALUE :].astype(BF16)

    project(near, ctx_rows)
    send_pair(1)
    send_pair(2)
    for step in range(first_steps + 1, lat_ring.half + 1):
        lat_ring.arrive_step(step)
    project(far, ctx_rows + near_rows)
    send_pair(3)

    def attend(chip):
        for piece in range(4):
            remote(
                pair_view(chip * 2 + 1 - core, piece),
                pair_view(chip * 2 + 1 - core, piece),
                x_across.at[0, 0, piece],
                x_recv.at[1, chip, piece],
                sibling,
            ).wait_recv()
        block = pairs[pl.ds(chip * 2, 2)]
        block = block.reshape(block.shape[0] * block.shape[1], block.shape[2])
        scores = lax.dot_general(
            queries[...].reshape(2 * count, VALUE),
            block[:, :VALUE],
            (((1,), (1,)), ((), ())),
            preferred_element_type=F32,
        )
        powers = jnp.exp(scores)
        sums[...] += jnp.dot(powers.astype(BF16), block[:, VALUE:], preferred_element_type=F32)
        totals[...] += jnp.sum(powers, axis=1, keepdims=True)

    @pl.loop(1, pair_ring.half + 2)
    def _(step):
        def arrive(piece):
            pair_ring.arrive(step, piece, True, send_pair_across)
            pair_ring.arrive(step, piece, False, send_pair_across)

        arrive(0)
        arrive(1)
        attend(pair_ring.source(step - 1, True))
        arrive(2)
        arrive(3)
        for weight_step in range(1, weight_ring.half):
            when(
                step == min(weight_step, pair_ring.half),
                lambda: weight_ring.arrive_step(weight_step, send_weight_across),
            )
        when(
            (step >= 2) & (step <= pair_ring.half),
            lambda: attend(pair_ring.source(step - 1, False)),
        )

    ratio = sums[...] / totals[...]
    difference = ratio[:count] - share[0] * ratio[count:]
    normed = difference * lax.rsqrt(
        jnp.mean(difference * difference, axis=1, keepdims=True) + head_eps
    )
    head_output = (normed * head_gain[...] * head_scale).astype(BF16)
    heads_out[...] = (
        jnp.dot(order[...], head_output, preferred_element_type=F32)
        .astype(BF16)
        .reshape(heads_out.shape)
    )
    heads_in[y] = heads_out[y]
    heads_exchange.start()

    weight_ring.arrive_step(weight_ring.half, send_weight_across)

    def moves(ring):
        for step in range(1, ring.half + 1):
            for piece in range(ring.pieces):
                for right in (True, False):
                    if ring.carries(step, piece, right):
                        yield step, piece, right

    for step, piece, right in moves(weight_ring):
        source = weight_ring.source(step, right)
        remote(
            out_weights.at[source, 1 - core, piece],
            out_weights.at[source, 1 - core, piece],
            w_across.at[0, 0, piece],
            w_recv.at[1, source, piece],
            sibling,
        ).wait_recv()
    heads_exchange.wait_recv()
    branch = jnp.dot(
        jnp.concatenate([heads_in[i] for i in range(ny)], axis=1),
        out_weights[...].reshape(ny * VALUE, width),
        preferred_element_type=F32,
    )
    for i in range(nz):
        rows_out[i] = branch[i * rows : (i + 1) * rows].astype(BF16)
    rows_in[z] = rows_out[z]
    rows_exchange.start()

    for exchange in (part_exchange, lat_exchange, line_exchange, all_exchange, heads_exchange):
        exchange.wait_send()
    for ring in (lat_ring, weight_ring, pair_ring):
        ring.wait_send()
    for step, piece, right in moves(weight_ring):
        weight_across(step, piece, right).wait_send()
    for piece in range(4):
        pair_across(0, piece, True).wait_send()
    for step, piece, right in moves(pair_ring):
        pair_across(step, piece, right).wait_send()

    rows_exchange.wait_recv()
    total = rows_in[0].astype(F32)
    for i in range(1, nz):
        total = total + rows_in[i].astype(F32)
    out[...] = (lat[...].astype(F32) + term(4) * total).astype(out.dtype)
    rows_exchange.wait_send()


def shards(
    sizes,
    latents,
    context,
    condition,
    context_condition,
    norm_gain,
    shift_weight,
    scale_weight,
    gate_weight,
    query_weight,
    key_weight,
    value_weight,
    subtract_share,
    head_gain,
    output_weight,
):
    nx, ny, nz = sizes
    nsp = 2 * nx
    rows, width = latents.shape
    line_rows = ny * rows
    count = nz * line_rows
    ctx_rows = context.shape[0]
    keys = count + ctx_rows
    tiles = ny * shift_weight.shape[1] // 128
    half = output_weight.shape[0] // 2
    vmem = pl.BlockSpec(memory_space=pltpu.VMEM)
    any_space = pl.BlockSpec(memory_space=pl.ANY)
    smem = pl.BlockSpec(memory_space=pltpu.SMEM)
    dma = pltpu.SemaphoreType.DMA
    hx, hy, hz = max(nx // 2, 1), max(ny // 2, 1), max(nz // 2, 1)
    scratch = [
        pltpu.VMEM((width, 3 * VALUE), BF16),
        pltpu.VMEM((ny, 2, 2, half // 2, width), BF16),
        pltpu.VMEM((8, 128), F32),
        pltpu.VMEM((nsp, 8, 128), F32),
        pltpu.VMEM((ny, 8, 128), F32),
        pltpu.VMEM((nz, tiles, 8, 128), F32),
        pltpu.VMEM((ny, rows, width), BF16),
        pltpu.VMEM((line_rows, width), F32),
        pltpu.VMEM((nz, line_rows, width), BF16),
        pltpu.VMEM((keys, width), BF16),
        pltpu.VMEM((nz, line_rows, VALUE), F32),
        pltpu.VMEM((nz, line_rows, VALUE), F32),
        pltpu.VMEM((nz, line_rows, VALUE), F32),
        pltpu.VMEM((count, count), BF16),
        pltpu.VMEM((2, nz, line_rows, VALUE), BF16),
        pltpu.VMEM((nsp, keys, 2 * VALUE), BF16),
        pltpu.VMEM((2 * count, VALUE), F32),
        pltpu.VMEM((2 * count, 1), F32),
        pltpu.VMEM((ny, nz * rows, VALUE), BF16),
        pltpu.VMEM((ny, nz * rows, VALUE), BF16),
        pltpu.VMEM((nz, rows, width), BF16),
        pltpu.VMEM((nz, rows, width), BF16),
        dma((7,)),
        dma((nsp,)),
        dma((nsp,)),
        dma((ny,)),
        dma((ny,)),
        dma((nz,)),
        dma((nz,)),
        dma((ny,)),
        dma((ny,)),
        dma((hz, 2)),
        dma((hz, 2)),
        dma((nz, 2)),
        dma((hy, 2)),
        dma((hy, 2)),
        dma((2, hy + 1, 2)),
        dma((2, ny, 2)),
        dma((hx, 4)),
        dma((hx, 4)),
        dma((2, hx + 1, 4)),
        dma((2, nx, 4)),
        dma((ny,)),
        dma((ny,)),
        dma((nz,)),
        dma((nz,)),
    ]
    return pl.pallas_call(
        functools.partial(kernel, sizes),
        out_shape=jax.ShapeDtypeStruct(latents.shape, latents.dtype),
        in_specs=[vmem] * 8 + [any_space] * 3 + [smem, vmem, any_space],
        out_specs=vmem,
        scratch_shapes=scratch,
        compiler_params=pltpu.CompilerParams(
            collective_id=0, has_side_effects=True, vmem_limit_bytes=48 * 2**20
        ),
    )(
        latents,
        context,
        condition.reshape(1, -1),
        context_condition.reshape(1, -1),
        norm_gain.reshape(1, -1),
        shift_weight,
        scale_weight,
        gate_weight,
        query_weight,
        key_weight,
        value_weight,
        subtract_share,
        head_gain.reshape(1, -1),
        output_weight,
    )


def solution(mesh):
    nsp, ntp = mesh.shape["sp"], mesh.shape["tp"]
    side = int(round(ntp**0.5))
    sizes = (nsp // 2, side, ntp // side)
    in_specs = (
        P(("sp", "tp"), None),
        P("sp", None),
        P("sp"),
        P("sp"),
        P(),
        P("sp", "tp"),
        P("sp", "tp"),
        P("sp", "tp"),
        P(None, "tp"),
        P(None, "tp"),
        P(None, "tp"),
        P("tp"),
        P(),
        P("tp", None),
    )
    out_specs = P(("sp", "tp"), None)
    return jax.shard_map(
        functools.partial(shards, sizes),
        mesh=mesh,
        in_specs=in_specs,
        out_specs=out_specs,
        check_vma=False,
    )
```

time: 221 us -> 90.2 us (0.41); the launches traced: 218 us -> 89.7 us
  waiting for transfers between devices: 111 us -> 0 us
  Pallas kernels: 0 us -> 81.1 us
  blocking collectives: 49.5 us -> 0 us
  starting transfers between devices: 18.7 us -> 0 us
  between operations: 14.4 us -> 0.71 us
  matrix products: 12 us -> 0 us
  other arithmetic: 4.76 us -> 0 us
    pallas_call x0 -> x1, Pallas kernels: none -> 81.1 us  [shards(): pl.pallas_call(functools.partial(kernel, sizes), out_shape=jax.ShapeDtype...]
    all_to_all x2 -> x0, waiting for transfers between devices: 73.1 us -> none  [the longest x1 49.8 us: sent_and_summed(): tiles = lax.all_to_all(split_up(array, dim, size), axis, 0, 0, tiled=True)]
    all_to_all x2 -> x0, blocking collectives: 49.5 us -> none  [copy_for_each(): lax.all_to_all(jnp.broadcast_to(array[None], (size, *array.shape)), axis,...]
    all_gather x1 -> x0, waiting for transfers between devices: 38.1 us -> none  [shards(): arrived = lax.all_gather(sent_pairs, 'sp', axis=0, tiled=True)]
    all_to_all x2 -> x0, starting transfers between devices: 18.6 us -> none  [the longest x1 13.8 us: sent_and_summed(): tiles = lax.all_to_all(split_up(array, dim, size), axis, 0, 0, tiled=True)]
    dot_general x10 -> x0, matrix products: 12 us -> none  [the longest x2 4.01 us: shards(): jnp.einsum('qd,kd->qk', queries[:, offset:offset + HEAD], arrived[:, offs...]
    unnamed x20 -> x30, local copies, waits for them, and re-layouts: 0.63 us -> 7.85 us
    broadcast_in_dim x3 -> x0, local copies, waits for them, and re-layouts: 2.34 us -> none  [copy_for_each(): jnp.broadcast_to(array[None], (size, *array.shape))]
  transfers between devices with their start and end apart: 3 -> 0, of which waited for: 3 -> 0; matrix products, arithmetic and copies ran while one was open for 1% -> 0% of each run, Pallas kernels for 0% -> 0%
where the time goes in v1:
time: 90.2 us; the launch traced here: 89.7 us
  Pallas kernels  81.1 us (90%)
  local copies, waits for them, and re-layouts  7.85 us (9%)
    pallas_call x1, Pallas kernels, shards(): pl.pallas_call(functools.partial(kernel, sizes), out_shape=jax.ShapeDtype...  81.1 us
    unnamed x30, local copies, waits for them, and re-layouts  7.85 us

profile of v1, /device:TPU:1, one launch (start us, length us, event | category | flops | bytes accessed | tf_op | source)
XLA Modules:
  0.0 89.7 jit_solution(2715359036056236005)
XLA Ops:
  0.0 0.0 copy-start.10
  0.7 0.0 copy-done.10
  0.7 0.0 copy-start.11
  0.7 0.1 copy.15.shift_w
  0.8 0.6 copy-done.11
  1.4 0.0 copy-start.12
  1.4 0.1 copy.16.scale_w
  1.5 0.6 copy-done.12
  2.1 0.0 copy-start.5
  2.1 0.0 copy-start.9
  2.1 0.1 copy.17.gate_w
  2.2 0.6 copy-done.5
  2.8 0.0 copy-done.6
  2.8 0.0 copy-done.7
  2.8 0.0 copy-done.8
  2.8 0.0 copy-done.9
  2.8 0.0 copy-start
  2.8 1.0 %copy-done = bf16[2048,128]{1,0:T(8,128)(2,1)S(1)} copy-done((bf16[2048,128]{1,0:T(8,128)(2,1)S(1)}, bf16[2048,128]{1,0:T(8,128)(2,1)}, u32[]{:S(2)}) %copy-start) | copy-done | bytes 524312
  3.9 1.0 %copy-done.1 = bf16[2048,128]{1,0:T(8,128)(2,1)S(1)} copy-done((bf16[2048,128]{1,0:T(8,128)(2,1)S(1)}, bf16[2048,128]{1,0:T(8,128)(2,1)}, u32[]{:S(2)}) %copy-start.1) | copy-done | bytes 524312
  4.9 1.0 %copy-done.2 = bf16[2048,128]{1,0:T(8,128)(2,1)S(1)} copy-done((bf16[2048,128]{1,0:T(8,128)(2,1)S(1)}, bf16[2048,128]{1,0:T(8,128)(2,1)}, u32[]{:S(2)}) %copy-start.2) | copy-done | bytes 524312
  6.0 1.0 %copy-done.3 = bf16[128,2048]{1,0:T(8,128)(2,1)S(1)} copy-done((bf16[128,2048]{1,0:T(8,128)(2,1)S(1)}, bf16[128,2048]{1,0:T(8,128)(2,1)}, u32[]{:S(2)}) %copy-start.3) | copy-done | bytes 524312
  7.0 0.9 %copy-done.4 = bf16[64,2048]{1,0:T(8,128)(2,1)S(1)} copy-done((bf16[64,2048]{1,0:T(8,128)(2,1)S(1)}, bf16[64,2048]{1,0:T(8,128)(2,1)}, u32[]{:S(2)}) %copy-start.4) | copy-done | bytes 262168
  7.9 81.1 %shard_map.136 = bf16[4,2048]{1,0:T(4,128)(2,1)S(1)} custom-call(bf16[4,2048]{1,0:T(4,128)(2,1)S(1)} %copy-done.5, bf16[64,2048]{1,0:T(8,128)(2,1)S(1)} %copy-done.4, f32[1,128]{1,0:T(1,128)S(1)} %bitcast.5, f32[1,128]{1,0:T(1,128)S(1)} %bitcast.6, f32[1,2048]{1,0:T(1,128)S(1)} %bitcast.4, bf16[128,32]{1,0:T(8,128)(2,1)S(1)} %copy.15.shift_w, ...), custom_call_target="tpu_custom_call" | custom-call | tf_op jit(solution)/shard_map/pallas_call | solution.py:675
  89.0 0.6 copy.20
  (7 shorter events, 0.0 us)
Async XLA Ops:
  0.0 0.7 copy-start.10
  0.7 0.7 copy-start.11
  1.4 0.7 copy-start.12
  2.1 0.7 copy-start.5
  2.1 0.7 copy-start.6
  2.1 0.7 copy-start.7
  2.1 0.7 copy-start.8
  2.1 0.7 copy-start.9
  2.8 1.0 %copy-start = (bf16[2048,128]{1,0:T(8,128)(2,1)S(1)}, bf16[2048,128]{1,0:T(8,128)(2,1)}, u32[]{:S(2)}) copy-start(bf16[2048,128]{1,0:T(8,128)(2,1)} %query_w.1) | copy-start | bytes 1572868
  3.9 1.0 %copy-start.1 = (bf16[2048,128]{1,0:T(8,128)(2,1)S(1)}, bf16[2048,128]{1,0:T(8,128)(2,1)}, u32[]{:S(2)}) copy-start(bf16[2048,128]{1,0:T(8,128)(2,1)} %key_w.1) | copy-start | bytes 1572868
  4.9 1.0 %copy-start.2 = (bf16[2048,128]{1,0:T(8,128)(2,1)S(1)}, bf16[2048,128]{1,0:T(8,128)(2,1)}, u32[]{:S(2)}) copy-start(bf16[2048,128]{1,0:T(8,128)(2,1)} %value_w.1) | copy-start | bytes 1572868
  6.0 1.0 %copy-start.3 = (bf16[128,2048]{1,0:T(8,128)(2,1)S(1)}, bf16[128,2048]{1,0:T(8,128)(2,1)}, u32[]{:S(2)}) copy-start(bf16[128,2048]{1,0:T(8,128)(2,1)} %out_w.1) | copy-start | bytes 1572868
  7.0 0.9 %copy-start.4 = (bf16[64,2048]{1,0:T(8,128)(2,1)S(1)}, bf16[64,2048]{1,0:T(8,128)(2,1)}, u32[]{:S(2)}) copy-start(bf16[64,2048]{1,0:T(8,128)(2,1)} %ctx.1) | copy-start | bytes 786436

commit v2 on v1

--- a/solution.py
+++ b/solution.py
@@ -142,7 +142,21 @@
 
 def kernel(
     sizes,
-    lat,
+    lat_hbm,
+    ctx_hbm,
+    cond_hbm,
+    ctx_cond_hbm,
+    gain_hbm,
+    shift_hbm,
+    scale_hbm,
+    gate_hbm,
+    query_w,
+    key_w,
+    value_w,
+    share_hbm,
+    head_gain_hbm,
+    out_w,
+    out,
     ctx,
     cond,
     ctx_cond,
@@ -150,13 +164,8 @@
     shift_w,
     scale_w,
     gate_w,
-    query_w,
-    key_w,
-    value_w,
+    head_gain,
     share,
-    head_gain,
-    out_w,
-    out,
     weights,
     out_weights,
     spread,
@@ -180,6 +189,7 @@
     rows_out,
     rows_in,
     local_sems,
+    early_sems,
     part_send,
     part_recv,
     line_send,
@@ -206,7 +216,7 @@
 ):
     nx, ny, nz = sizes
     nsp = 2 * nx
-    rows, width = lat.shape
+    rows, width = lat_hbm.shape
     line_rows = ny * rows
     count = nz * line_rows
     ctx_rows = ctx.shape[0]
@@ -227,6 +237,22 @@
 
     def on_z(peer):
         return {"sp": sp, "tp": peer * ny + y}
+
+    early = [
+        pltpu.make_async_copy(source, place, early_sems.at[i])
+        for i, (source, place) in enumerate(
+            (
+                (cond_hbm, cond),
+                (ctx_cond_hbm, ctx_cond),
+                (shift_hbm, shift_w),
+                (scale_hbm, scale_w),
+                (gate_hbm, gate_w),
+                (lat_hbm, lat_line.at[y]),
+            )
+        )
+    ]
+    for copy in early:
+        copy.start()
 
     barrier = pltpu.get_barrier_semaphore()
     for me, size, device_of in ((sp, nsp, on_sp), (y, ny, on_y), (z, nz, on_z)):
@@ -253,22 +279,32 @@
                     local_sems.at[3 + 2 * half + piece],
                 )
             )
+    local.append(pltpu.make_async_copy(ctx_hbm, ctx, local_sems.at[7]))
+    local.append(pltpu.make_async_copy(gain_hbm, gain, local_sems.at[8]))
+    local.append(pltpu.make_async_copy(head_gain_hbm, head_gain, local_sems.at[9]))
+    local.append(pltpu.make_async_copy(share_hbm, share, local_sems.at[10]))
     for copy in local:
         copy.start()
-
-    columns = shift_w.shape[1]
+    for copy in early:
+        copy.wait()
+
+    columns = shift_w.shape[0]
     group = 128 // columns
     tiles = ny // group
     raw = jnp.where(iota((8, cond.shape[1]), 0) == 0, cond[...], ctx_cond[...])
     activated = (raw / (1.0 + jnp.exp(-raw))).astype(BF16)
     spread[...] = jnp.zeros_like(spread)
     for kind, matrix in enumerate((shift_w, scale_w, gate_w)):
-        term = jnp.dot(activated, matrix[...], preferred_element_type=F32)[0:2]
+        term = lax.dot_general(
+            activated,
+            matrix[...],
+            (((1,), (1,)), ((), ())),
+            preferred_element_type=F32,
+        )[0:2]
         for place in range(group):
             spread[2 * kind : 2 * kind + 2, place * columns : (place + 1) * columns] = term
     here = iota((8, 128), 1) // columns == lax.rem(y, group)
     part[sp] = jnp.where(here, spread[...], 0.0)
-    lat_line[y] = lat[...]
 
     pl.semaphore_wait(barrier, nsp - 1 + ny - 1 + nz - 1)
 
@@ -276,7 +312,7 @@
         sp, nsp, on_sp, lambda peer: part.at[sp], lambda me: part.at[me], part_send, part_recv
     )
     lat_exchange = Exchange(
-        y, ny, on_y, lambda peer: lat, lambda me: lat_line.at[me], lat_send, lat_recv
+        y, ny, on_y, lambda peer: lat_line.at[y], lambda me: lat_line.at[me], lat_send, lat_recv
     )
     line_exchange = Exchange(
         y,
@@ -302,13 +338,13 @@
     rows_exchange = Exchange(
         z, nz, on_z, lambda peer: rows_out.at[peer], lambda me: rows_in.at[me], rows_send, rows_recv
     )
-    half_line = line_rows // 2
+    part_line = line_rows // 4
     lat_ring = Ring(
         z,
         nz,
         on_z,
-        lambda source, piece: lat_all.at[source, pl.ds(piece * half_line, half_line)],
-        2,
+        lambda source, piece: lat_all.at[source, pl.ds(piece * part_line, part_line)],
+        4,
         z_right,
         z_left,
         z_recv,
@@ -336,6 +372,14 @@
 
     def send_weight_across(step, piece, right):
         weight_across(step, piece, right).start()
+
+    weight_moves = [(step, piece) for step in range(1, weight_ring.half + 1) for piece in range(2)]
+
+    def pass_weights(index):
+        if index < len(weight_moves):
+            step, piece = weight_moves[index]
+            weight_ring.arrive(step, piece, True, send_weight_across)
+            weight_ring.arrive(step, piece, False, send_weight_across)
 
     near = [0]
     for step in range(1, lat_ring.half // 2 + 1):
@@ -418,7 +462,7 @@
     for i in range(ny):
         lat_flat[i * rows : (i + 1) * rows, :] = lat_line[i].astype(F32)
     lat_all[z] = lat_flat[...].astype(BF16)
-    for piece in range(2):
+    for piece in range(4):
         lat_ring.send_own(piece)
 
     for copy in local:
@@ -439,6 +483,7 @@
         lat_ring.arrive_step(step)
 
     all_exchange.wait_recv()
+    pass_weights(0)
 
     def term(row):
         return jnp.concatenate(
@@ -484,10 +529,12 @@
     project(near, ctx_rows)
     send_pair(1)
     send_pair(2)
+    pass_weights(1)
     for step in range(first_steps + 1, lat_ring.half + 1):
         lat_ring.arrive_step(step)
     project(far, ctx_rows + near_rows)
     send_pair(3)
+    pass_weights(2)
 
     def attend(chip):
         for piece in range(4):
@@ -518,21 +565,15 @@
 
         arrive(0)
         arrive(1)
-        attend(pair_ring.source(step - 1, True))
+        pl.when(step >= 2)(lambda: attend(pair_ring.source(step - 1, True)))
         arrive(2)
         arrive(3)
-        for weight_step in range(1, weight_ring.half):
-            when(
-                step == min(weight_step, pair_ring.half),
-                lambda: weight_ring.arrive_step(weight_step, send_weight_across),
-            )
-        when(
-            (step >= 2) & (step <= pair_ring.half),
-            lambda: attend(pair_ring.source(step - 1, False)),
-        )
+        for index in (3, 4, 5):
+            pl.when(step == min(index - 2, pair_ring.half))(lambda: pass_weights(index))
+        pl.when(step <= pair_ring.half)(lambda: attend(pair_ring.source(step - 1, False)))
 
     ratio = sums[...] / totals[...]
-    difference = ratio[:count] - share[0] * ratio[count:]
+    difference = ratio[:count] - share[...] * ratio[count:]
     normed = difference * lax.rsqrt(
         jnp.mean(difference * difference, axis=1, keepdims=True) + head_eps
     )
@@ -545,7 +586,8 @@
     heads_in[y] = heads_out[y]
     heads_exchange.start()
 
-    weight_ring.arrive_step(weight_ring.half, send_weight_across)
+    pass_weights(6)
+    pass_weights(7)
 
     def moves(ring):
         for step in range(1, ring.half + 1):
@@ -589,7 +631,7 @@
     total = rows_in[0].astype(F32)
     for i in range(1, nz):
         total = total + rows_in[i].astype(F32)
-    out[...] = (lat[...].astype(F32) + term(4) * total).astype(out.dtype)
+    out[...] = (lat_line[y].astype(F32) + term(4) * total).astype(out.dtype)
     rows_exchange.wait_send()
 
 
@@ -621,10 +663,18 @@
     half = output_weight.shape[0] // 2
     vmem = pl.BlockSpec(memory_space=pltpu.VMEM)
     any_space = pl.BlockSpec(memory_space=pl.ANY)
-    smem = pl.BlockSpec(memory_space=pltpu.SMEM)
     dma = pltpu.SemaphoreType.DMA
     hx, hy, hz = max(nx // 2, 1), max(ny // 2, 1), max(nz // 2, 1)
     scratch = [
+        pltpu.VMEM(context.shape, BF16),
+        pltpu.VMEM((1, condition.size), F32),
+        pltpu.VMEM((1, condition.size), F32),
+        pltpu.VMEM((1, width), F32),
+        pltpu.VMEM(shift_weight.shape[::-1], BF16),
+        pltpu.VMEM(shift_weight.shape[::-1], BF16),
+        pltpu.VMEM(shift_weight.shape[::-1], BF16),
+        pltpu.VMEM((1, VALUE), F32),
+        pltpu.VMEM((1, 1), F32),
         pltpu.VMEM((width, 3 * VALUE), BF16),
         pltpu.VMEM((ny, 2, 2, half // 2, width), BF16),
         pltpu.VMEM((8, 128), F32),
@@ -647,7 +697,8 @@
         pltpu.VMEM((ny, nz * rows, VALUE), BF16),
         pltpu.VMEM((nz, rows, width), BF16),
         pltpu.VMEM((nz, rows, width), BF16),
-        dma((7,)),
+        dma((11,)),
+        dma((6,)),
         dma((nsp,)),
         dma((nsp,)),
         dma((ny,)),
@@ -656,9 +707,9 @@
         dma((nz,)),
         dma((ny,)),
         dma((ny,)),
-        dma((hz, 2)),
-        dma((hz, 2)),
-        dma((nz, 2)),
+        dma((hz, 4)),
+        dma((hz, 4)),
+        dma((nz, 4)),
         dma((hy, 2)),
         dma((hy, 2)),
         dma((2, hy + 1, 2)),
@@ -675,11 +726,11 @@
     return pl.pallas_call(
         functools.partial(kernel, sizes),
         out_shape=jax.ShapeDtypeStruct(latents.shape, latents.dtype),
-        in_specs=[vmem] * 8 + [any_space] * 3 + [smem, vmem, any_space],
+        in_specs=[any_space] * 14,
         out_specs=vmem,
         scratch_shapes=scratch,
         compiler_params=pltpu.CompilerParams(
-            collective_id=0, has_side_effects=True, vmem_limit_bytes=48 * 2**20
+            collective_id=0, has_side_effects=True, vmem_limit_bytes=67043328
         ),
     )(
         latents,
@@ -687,13 +738,13 @@
         condition.reshape(1, -1),
         context_condition.reshape(1, -1),
         norm_gain.reshape(1, -1),
-        shift_weight,
-        scale_weight,
-        gate_weight,
+        shift_weight.T,
+        scale_weight.T,
+        gate_weight.T,
         query_weight,
         key_weight,
         value_weight,
-        subtract_share,
+        subtract_share.reshape(1, 1),
         head_gain.reshape(1, -1),
         output_weight,
     )

time: 90.2 us -> 78.4 us (0.87)
  local copies, waits for them, and re-layouts: 7.85 us -> 1.33 us
  Pallas kernels: 81.1 us -> 76.2 us
    unnamed x30 -> x1, local copies, waits for them, and re-layouts: 7.85 us -> 1.33 us
    pallas_call x1, Pallas kernels: 81.1 us -> 76.2 us  [shards(): pl.pallas_call(functools.partial(kernel, sizes), out_shape=jax.ShapeDtype...]
where the time goes in v2:
time: 78.4 us; the launch traced here: 78.2 us
  Pallas kernels  76.2 us (97%)
  local copies, waits for them, and re-layouts  1.33 us (2%)
    pallas_call x1, Pallas kernels, shards(): pl.pallas_call(functools.partial(kernel, sizes), out_shape=jax.ShapeDtype...  76.2 us

profile of v2, /device:TPU:1, one launch (start us, length us, event | category | flops | bytes accessed | tf_op | source)
XLA Modules:
  0.0 78.2 jit_solution(13218443401302248460)
XLA Ops:
  0.7 76.2 %shard_map.136 = bf16[4,2048]{1,0:T(4,128)(2,1)} custom-call(bf16[4,2048]{1,0:T(4,128)(2,1)} %lat_hbm.1, bf16[64,2048]{1,0:T(8,128)(2,1)} %ctx_hbm.1, f32[1,128]{1,0:T(1,128)} %bitcast.13, f32[1,128]{1,0:T(1,128)} %bitcast.14, f32[1,2048]{1,0:T(1,128)} %bitcast.9, bf16[32,128]{1,0:T(8,128)(2,1)} %bitcast.10, bf16[32,128]{1,0:T(8,128)(2,1)} %bitcast.11, ...), custom_call_target="tpu_custom_call" | custom-call | tf_op jit(solution)/shard_map/pallas_call | solution.py:726
  76.8 1.3 %copy.17 = bf16[4,2048]{1,0:T(4,128)(2,1)} copy(bf16[4,2048]{1,0:T(4,128)(2,1)} %shard_map.136) | data formatting | bytes 32768
